TPU v7x, 128 devices: a whole 4x4x4 slice. The times are simulated.
128 devices in a mesh: rep: 2 (over z_hi), fs: 32 (over z_lo, y, x), tp: 2 (over core).
Axes of the slice: x: 4, y: 4, z: 4 (z_hi: 2, z_lo: 2; z = z_hi * 2 + z_lo), core: 2. Of those that a mesh axis runs over, the one named last changes fastest.
Arguments:
- tokens: bfloat16 [49152, 2048], P(('rep', 'fs'), 'tp'), may hold values from -6 to 6
- first_norm_gain: bfloat16 [2048], replicated, may hold values from 0.099609375 to 1.8984375
- query_projection_weight: bfloat16 [2048, 512], P('fs', 'tp'), may hold values from -0.125 to 0.125
- key_projection_weight: bfloat16 [2048, 512], P('fs', 'tp'), may hold values from -0.125 to 0.125
- value_projection_weight: bfloat16 [2048, 1024], P('fs', 'tp'), may hold values from -0.125 to 0.125
- output_gate_weight: bfloat16 [2048, 1024], P('fs', 'tp'), may hold values from -0.125 to 0.125
- decay_projection_weight: bfloat16 [2048, 512], P('fs', 'tp'), may hold values from -0.375 to 0.375
- fading_shift_vector: float32 [512], P('tp'), may hold values from -1 to 4
- added_fading_exponent: float32 [49152, 512], P(('rep', 'fs'), 'tp'), may hold values from -0.7 to 0
- per_head_gain: bfloat16 [128], replicated, may hold values from 0.099609375 to 1.8984375
- mixer_result_matrix: bfloat16 [1024, 2048], P('tp', 'fs'), may hold values from -0.1875 to 0.1875
- second_norm_gain: bfloat16 [2048], replicated, may hold values from 0.099609375 to 1.8984375
- up_linear_weight: bfloat16 [2048, 3072], P('fs', 'tp'), may hold values from -0.125 to 0.125
- up_gating_weight: bfloat16 [2048, 3072], P('fs', 'tp'), may hold values from -0.125 to 0.125
- depthwise_taps: bfloat16 [2, 3, 3072], P(None, None, 'tp'), may hold values from -3.5 to 3.5
- depthwise_bias: bfloat16 [2, 3072], P(None, 'tp'), may hold values from -3 to 3
- down_projection_weight: bfloat16 [3072, 2048], P('tp', 'fs'), may hold values from -0.109375 to 0.109375
Outputs:
- mixed: bfloat16 [49152, 2048], P(('rep', 'fs'), 'tp')
All inputs are finite; a program needn't handle non-finite values.
Results may differ from a plain program's by a relative error of at most 0.018.
Values may be sent and summed in bfloat16 or wider, within the bound.
A program may use at most 128 MiB of HBM per device.

v0:
```python
import jax
import jax.numpy as jnp
from jax import lax
from jax.experimental import pallas as pl
from jax.experimental.pallas import tpu as pltpu
from jax.sharding import PartitionSpec as P

LANE = 128
MESH = pl.DeviceIdType.MESH
GROUPS = ((0, (6, 5, 3, 4)), (18, (7, 8, 5, 4)), (42, (4, 4, 2, 2)))
COLS = 54 * LANE
CLASSES = (("x", 1, True), ("y", -1, True), ("x", 1, False), ("y", -1, False))
NSEM = 144


class Gather:
    def __init__(self, full, send_sem, recv_sem):
        self.full, self.send_sem, self.recv_sem = full, send_sem, recv_sem
        rep, fs, self.tp = (lax.axis_index(a) for a in ("rep", "fs", "tp"))
        self.x, self.y, self.l = lax.rem(fs, 4), lax.rem(fs // 4, 4), fs // 16
        self.z = rep * 2 + self.l
        self.ids, self.sent = {}, {}

    def device(self, dim, step):
        x, y, z = self.x, self.y, self.z
        if dim == "x":
            x = lax.rem(x + step + 4, 4)
        elif dim == "y":
            y = lax.rem(y + step + 4, 4)
        else:
            z = lax.rem(z + step + 4, 4)
        return (z // 2, lax.rem(z, 2) * 16 + y * 4 + x, self.tp)

    def neighbours(self):
        return [self.device(d, s) for d in "xyz" for s in (1, -1)] + [
            (self.z // 2, self.l * 16 + self.y * 4 + self.x, 1 - self.tp)
        ]

    def cols(self, g, c):
        at, widths = GROUPS[g]
        return pl.ds((at + sum(widths[:c])) * LANE, widths[c] * LANE)

    def piece(self, g, c, stage, off, half=None, z=None):
        first, _, last = CLASSES[c]
        if z is None:
            zs = pl.ds(self.l, 1) if last else pl.ds(0, 2)
        else:
            zs = pl.ds(z, 1)
        rows = pl.ds(0, 64) if half is None else pl.ds(32 * half, 32)
        dim = first if stage == 1 else ("y" if first == "x" else "x")
        mine = self.x if dim == "x" else self.y
        at = pl.ds(lax.rem(mine + off + 4, 4), 1)
        if stage == 1:
            other = pl.ds(self.y if dim == "x" else self.x, 1)
        else:
            other = pl.ds(0, 4)
        yx = (other, at) if dim == "x" else (at, other)
        return self.full.at[zs, yx[0], yx[1], rows, self.cols(g, c)]

    def copy(self, key, ref, dim, step):
        i = self.ids.setdefault(key, len(self.ids))
        return pltpu.make_async_remote_copy(
            src_ref=ref,
            dst_ref=ref,
            send_sem=self.send_sem.at[i],
            recv_sem=self.recv_sem.at[i],
            device_id=self.device(dim, step),
            device_id_type=MESH,
        )

    def send(self, key, ref_args, dim, step):
        copy = self.copy(key, self.piece(*ref_args), dim, step)
        copy.start()
        self.sent[key] = (ref_args, dim, step)

    def recv(self, key, ref):
        self.copy(key, ref, "x", 1).wait_recv()

    def dim(self, c, stage):
        first = CLASSES[c][0]
        return first if stage == 1 else ("y" if first == "x" else "x")

    def hop_one(self, g, c, stage):
        own = (g, c, stage, 0)
        self.send((g, c, stage, "f1"), own, self.dim(c, stage), 1)
        self.send((g, c, stage, "b1"), own, self.dim(c, stage), -1)

    def hop_two(self, g, c, stage):
        d = self.dim(c, stage)
        self.recv((g, c, stage, "f1"), self.piece(g, c, stage, -1))
        self.send((g, c, stage, "f2"), (g, c, stage, -1, 0), d, 1)
        self.recv((g, c, stage, "b1"), self.piece(g, c, stage, 1))
        self.send((g, c, stage, "b2"), (g, c, stage, 1, 1), d, -1)

    def hop_end(self, g, c, stage):
        self.recv((g, c, stage, "f2"), self.piece(g, c, stage, 2, 0))
        self.recv((g, c, stage, "b2"), self.piece(g, c, stage, 2, 1))

    def zkey(self, g, c, stage, off):
        return (g, c, stage, "z", off)

    def zsend(self, g, c, stage, off):
        self.send(
            self.zkey(g, c, stage, off),
            (g, c, stage, off, None, self.l),
            "z",
            CLASSES[c][1],
        )

    def zrecv(self, g, c, stage, off):
        self.recv(
            self.zkey(g, c, stage, off), self.piece(g, c, stage, off, z=1 - self.l)
        )

    def step(self, g, s):
        if s == 0:
            for c in (0, 1):
                self.hop_one(g, c, 1)
            for c in (2, 3, 0, 1):
                self.zsend(g, c, 1, 0)
        elif s == 1:
            for c in (2, 3):
                self.zrecv(g, c, 1, 0)
                self.hop_one(g, c, 1)
        elif s in (2, 6):
            stage = 1 if s == 2 else 2
            for c in (0, 1):
                self.hop_two(g, c, stage)
                self.zsend(g, c, stage, -1)
                self.zsend(g, c, stage, 1)
        elif s in (3, 7):
            for c in (2, 3):
                self.hop_two(g, c, 1 if s == 3 else 2)
        elif s in (4, 8):
            stage = 1 if s == 4 else 2
            for c in (0, 1):
                self.hop_end(g, c, stage)
                if stage == 1:
                    self.hop_one(g, c, 2)
                self.zsend(g, c, stage, 2)
        elif s == 5:
            for c in (2, 3):
                self.hop_end(g, c, 1)
                self.hop_one(g, c, 2)
        elif s == 9:
            for c in (2, 3):
                self.hop_end(g, c, 2)
            for c in (0, 1):
                for stage, off in ((1, 0), (1, -1), (1, 1), (1, 2), (2, -1), (2, 1), (2, 2)):
                    self.zrecv(g, c, stage, off)

    def enter(self):
        barrier = pltpu.get_barrier_semaphore()
        for d in self.neighbours():
            pl.semaphore_signal(barrier, inc=1, device_id=d, device_id_type=MESH)
        pl.semaphore_wait(barrier, 7)

    def partner(self):
        return (self.z // 2, self.l * 16 + self.y * 4 + self.x, 1 - self.tp)

    def steps(self, todo):
        for g, s in todo:
            self.step(g, s)

    def steps_in(self, i, plan):
        for at, todo in plan.items():

            @pl.when(i == at)
            def _():
                self.steps(todo)

    def leave(self):
        for key, (ref_args, dim, step) in self.sent.items():
            self.copy(key, self.piece(*ref_args), dim, step).wait_send()


ROWS = 768
SEQ = 256
HALF = 1024
NORM_EPS = 1e-06
SHARPNESS = 16.0
MIX_AT, UP_AT, DOWN_AT, FF = 1792, 2304, 5376, 1536
ROW_STEP = 16
F32, BF16 = jnp.float32, jnp.bfloat16

PLAN = {
    "open": [(0, 0)],
    "tokens": [(0, 1)],
    "norm": {8: [(0, 2)], 16: [(0, 3)], 32: [(0, 4), (0, 5), (1, 0)]},
    "first": [(0, 6), (1, 1), (0, 7), (0, 8), (1, 2), (1, 3), (1, 4), (1, 5), (0, 9), (2, 0)],
    "project": {5: [(1, 6), (2, 1)]},
    "heads": {1: [(1, 7)], 3: [(2, 2)]},
    "mix": {1: [(1, 8), (2, 3)], 5: [(2, 4)]},
    "second": {0: [(2, 5)]},
    "up_first": [(1, 9)],
    "up": {1: [(2, 6)], 3: [(2, 7)], 4: [(2, 8)]},
    "last": [(2, 9)],
}


def dot(a, b):
    return jnp.dot(a, b, preferred_element_type=F32)


def dot_nt(a, b):
    return lax.dot_general(a, b, (((1,), (1,)), ((), ())), preferred_element_type=F32)


def normalize(parts, gain_ref):
    total = sum(jnp.sum(p * p, axis=-1, keepdims=True) for p in parts)
    scale = lax.rsqrt(total * (1.0 / 2048) + NORM_EPS)
    width = 2048 // len(parts)
    return [
        (p * scale * gain_ref[:, i * width : (i + 1) * width].astype(F32)).astype(BF16)
        for i, p in enumerate(parts)
    ]


def head_pair(s, pair, qkvg, decay, mixed, head_gain):
    rows = pl.ds(pl.multiple_of(s * SEQ, SEQ), SEQ)
    at = pl.multiple_of(pair * LANE, LANE)
    lane = lax.broadcasted_iota(jnp.int32, (1, LANE), 1)
    low = lane < 64
    t = lax.broadcasted_iota(jnp.int32, (SEQ, SEQ), 0)
    u = lax.broadcasted_iota(jnp.int32, (SEQ, SEQ), 1)
    before = u <= t
    after = u >= t

    log_a = decay[rows, pl.ds(at, LANE)]
    ones = before.astype(F32).astype(BF16)
    high = log_a.astype(BF16)
    rest = log_a - high.astype(F32)
    middle = rest.astype(BF16)
    small = (rest - middle.astype(F32)).astype(BF16)
    done = dot(ones, high) + (dot(ones, middle) + dot(ones, small))
    open_ = done - log_a
    mid = [done[64 * b + 31 : 64 * b + 32] for b in range(4)]
    mid_open = [open_[64 * b + 32 : 64 * b + 33] for b in range(4)]

    q = qkvg[rows, pl.ds(at, LANE)].astype(F32) * 0.125
    k = qkvg[rows, pl.ds(pl.multiple_of(at + 256, LANE), LANE)].astype(F32)
    blocks = [slice(64 * b, 64 * b + 64) for b in range(4)]
    key_fwd = [k[r] * jnp.exp(mid[b] - done[r]) for b, r in enumerate(blocks)]
    key_bwd = [k[r] * jnp.exp(open_[r] - mid_open[b]) for b, r in enumerate(blocks)]

    def swap(v):
        return pltpu.roll(v, 64, 1)

    def both(v, parity):
        other = swap(v)
        return jnp.where(low, v, other) if parity == 0 else jnp.where(low, other, v)

    nothing = jnp.zeros((64, LANE), BF16)

    def side(queries, points, mids, keys, backward, parity):
        sign = -1.0 if backward else 1.0
        point_mids = [
            jnp.where(low, both(mids[2 * p], parity), both(mids[2 * p + 1], parity))
            for p in range(2)
        ]
        left, right = [], []
        for b, r in enumerate(blocks):
            row = []
            for p in range(2):
                expo = (points[r] - point_mids[p]) * sign
                if backward:
                    used = (b <= 2 * p, b <= 2 * p + 1)
                else:
                    used = (b >= 2 * p, b >= 2 * p + 1)
                if not any(used):
                    row.append(nothing)
                    continue
                if not all(used):
                    expo = jnp.where(low if used[0] else ~low, expo, -1e30)
                row.append((queries[r] * jnp.exp(expo)).astype(BF16))
            left.append(jnp.concatenate(row, axis=1))
            mine = keys[b] if parity == b % 2 else swap(keys[b])
            mine = jnp.where(low if b % 2 == 0 else ~low, mine, 0.0).astype(BF16)
            right.append(
                jnp.concatenate([mine if p == b // 2 else nothing for p in range(2)], axis=1)
            )
        return dot_nt(jnp.concatenate(left, axis=0), jnp.concatenate(right, axis=0))

    for parity in range(2):
        queries = both(q, parity)
        fwd = side(queries, both(done, parity), mid, key_fwd, False, parity)
        bwd = side(queries, both(open_, parity), mid_open, key_bwd, True, parity)
        scores = jnp.where(before, fwd, 0.0) + jnp.where(after, bwd, 0.0)
        place = pl.multiple_of(pair * 256 + parity * LANE, LANE)
        values = qkvg[rows, pl.ds(pl.multiple_of(place + 512, LANE), LANE)]
        out = dot(scores.astype(BF16), values)
        scale = lax.rsqrt(jnp.mean(out * out, axis=-1, keepdims=True) + NORM_EPS)
        out = out * scale * head_gain[...].astype(F32)
        gate = qkvg[rows, pl.ds(pl.multiple_of(place + 1024, LANE), LANE)].astype(F32)
        out = out * (gate * jax.nn.sigmoid(gate))
        mixed[rows, pl.ds(place, LANE)] = out.astype(BF16)


def smooth(source, taps, bias):
    row = lax.broadcasted_iota(jnp.int32, source.shape, 0)
    back = jnp.where(row == 0, 0.0, pltpu.roll(source, 1, 0))
    ahead = jnp.where(row == SEQ - 1, 0.0, pltpu.roll(source, SEQ - 1, 0))
    return bias + back * taps[0:1] + source * taps[1:2] + ahead * taps[2:3]


def layer_kernel(
    tokens,
    wq,
    wk,
    wv,
    wg,
    wd,
    mix_t,
    up_lin,
    up_gate,
    down_t,
    added,
    gain_one,
    shift,
    head_gain,
    gain_two,
    taps,
    bias,
    out,
    full,
    tok,
    normed,
    qkvg,
    decay,
    fading,
    mixed,
    mix_out,
    mix_in,
    hidden,
    down_out,
    down_in,
    result,
    send_sem,
    recv_sem,
    load_sem,
    pair_send,
    pair_recv,
    out_sem,
):
    g = Gather(full, send_sem, recv_sem)
    tp = g.tp
    own = full.at[g.l, g.y, g.x]
    loads = [pltpu.make_async_copy(tokens, tok.at[tp], load_sem.at[0])]
    at = 0
    for n, w in enumerate((wq, wk, wv, wg, wd, mix_t, up_lin, up_gate, down_t)):
        width = w.shape[1]
        loads.append(
            pltpu.make_async_copy(w, own.at[:, pl.ds(at, width)], load_sem.at[n + 1])
        )
        at += width
    fading_load = pltpu.make_async_copy(added, fading, load_sem.at[10])
    for load in loads:
        load.start()
    fading_load.start()
    g.enter()

    def to_partner(src, dst, n):
        return pltpu.make_async_remote_copy(
            src_ref=src,
            dst_ref=dst,
            send_sem=pair_send.at[n],
            recv_sem=pair_recv.at[n],
            device_id=g.partner(),
            device_id_type=MESH,
        )

    for load in loads[1:7]:
        load.wait()
    for load in loads[7:]:
        load.wait()
    g.steps(PLAN["open"])
    loads[0].wait()
    swap_tokens = to_partner(tok.at[tp], tok.at[tp], 0)
    swap_tokens.start()
    fading_load.wait()
    g.steps(PLAN["tokens"])
    to_partner(tok.at[tp], tok.at[1 - tp], 0).wait_recv()

    def first_norm(i, _):
        rows = pl.ds(pl.multiple_of(i * ROW_STEP, ROW_STEP), ROW_STEP)
        parts = normalize([tok[h, rows, :].astype(F32) for h in range(2)], gain_one)
        for h in range(2):
            normed[rows, h * HALF : (h + 1) * HALF] = parts[h]
        g.steps_in(i, PLAN["norm"])
        return 0

    lax.fori_loop(0, ROWS // ROW_STEP, first_norm, 0)
    g.steps(PLAN["first"])

    score = dot(normed[...], full[:, :, :, :, 1536:1792].reshape(2048, 256)) + shift[...]
    faded = jnp.minimum(score, 0.0) - jnp.log1p(jnp.exp(-jnp.abs(score)))
    decay[...] = faded * (1.0 / SHARPNESS) + fading[...]

    def project(j, _):
        cols = pl.ds(pl.multiple_of(j * 256, 256), 256)
        weight = full[:, :, :, :, cols].reshape(2048, 256)
        qkvg[:, cols] = dot(normed[...], weight).astype(BF16)
        g.steps_in(j, PLAN["project"])
        return 0

    lax.fori_loop(0, 6, project, 0)

    def heads(i, _):
        head_pair(i // 2, lax.rem(i, 2), qkvg, decay, mixed, head_gain)
        g.steps_in(i, PLAN["heads"])
        return 0

    lax.fori_loop(0, 6, heads, 0)

    def mix(j, _):
        weight = full[j // 4, lax.rem(j, 4), :, :, MIX_AT:UP_AT].reshape(256, 512)
        mix_out[j] = dot_nt(mixed[...], weight).astype(BF16)
        to_partner(mix_out.at[j], mix_in.at[j], 1 + j).start()
        g.steps_in(j, PLAN["mix"])
        return 0

    lax.fori_loop(0, 8, mix, 0)
    for j in range(8):
        to_partner(mix_out.at[j], mix_in.at[j], 1 + j).wait_recv()

    def second_norm(i, _):
        rows = pl.ds(pl.multiple_of(i * ROW_STEP, ROW_STEP), ROW_STEP)
        parts = []
        for j in range(8):
            cols = slice((j % 4) * 256, (j % 4 + 1) * 256)
            term = mix_out[j, rows, :].astype(F32) + mix_in[j, rows, :].astype(F32)
            kept = (tok[j // 4, rows, cols].astype(F32) + term).astype(BF16)
            tok[j // 4, rows, cols] = kept
            parts.append(kept.astype(F32))
        for j, part in enumerate(normalize(parts, gain_two)):
            normed[rows, j * 256 : (j + 1) * 256] = part
        g.steps_in(i, PLAN["second"])
        return 0

    swap_tokens.wait_send()
    lax.fori_loop(0, ROWS // ROW_STEP, second_norm, 0)
    g.steps(PLAN["up_first"])

    def up(j, _):
        cols = pl.ds(pl.multiple_of(j * 256, 256), 256)
        parts = []
        for half in range(2):
            at = pl.multiple_of(UP_AT + half * FF + j * 256, 256)
            weight = full[:, :, :, :, pl.ds(at, 256)].reshape(2048, 256)
            parts.append(dot(normed[...], weight).astype(BF16))
        tap = [taps[half, :, cols].astype(F32) for half in range(2)]
        base = bias[:, cols].astype(F32)
        for s in range(ROWS // SEQ):
            rows = slice(s * SEQ, (s + 1) * SEQ)
            lin, gate = (
                smooth(parts[h][rows].astype(F32), tap[h], base[h : h + 1]) for h in range(2)
            )
            hidden[rows, cols] = (lin * (gate * jax.nn.sigmoid(gate))).astype(BF16)
        g.steps_in(j, PLAN["up"])
        return 0

    lax.fori_loop(0, FF // 256, up, 0)
    g.steps(PLAN["last"])

    def down_part(half, j):
        weight = full[half, j, :, :, DOWN_AT:COLS].reshape(256, FF)
        return dot_nt(hidden[...], weight).astype(BF16)

    def down_theirs(j, _):
        down_out[j] = down_part(1 - tp, j)
        to_partner(down_out.at[j], down_in.at[j], 9 + j).start()
        return 0

    lax.fori_loop(0, 4, down_theirs, 0)

    def stored(j):
        return pltpu.make_async_copy(
            result.at[j],
            out.at[:, pl.ds(pl.multiple_of(j * 256, 256), 256)],
            out_sem.at[j],
        )

    def down_mine(j, _):
        mine = down_part(tp, j).astype(F32)
        to_partner(down_out.at[j], down_in.at[j], 9 + j).wait_recv()
        cols = pl.ds(pl.multiple_of(j * 256, 256), 256)
        summed = mine + down_in[j].astype(F32)
        result[j] = (tok[tp, :, cols].astype(F32) + summed).astype(BF16)
        stored(j).start()
        return 0

    lax.fori_loop(0, 4, down_mine, 0)
    for j in range(8):
        to_partner(mix_out.at[j], mix_in.at[j], 1 + j).wait_send()
    for j in range(4):
        to_partner(down_out.at[j], down_in.at[j], 9 + j).wait_send()
        stored(j).wait()
    g.leave()


def local(
    tokens,
    first_norm_gain,
    query_projection_weight,
    key_projection_weight,
    value_projection_weight,
    output_gate_weight,
    decay_projection_weight,
    fading_shift_vector,
    added_fading_exponent,
    per_head_gain,
    mixer_result_matrix,
    second_norm_gain,
    up_linear_weight,
    up_gating_weight,
    depthwise_taps,
    depthwise_bias,
    down_projection_weight,
):
    any_spec = pl.BlockSpec(memory_space=pl.ANY)
    vmem_spec = pl.BlockSpec(memory_space=pltpu.VMEM)
    dma = pltpu.SemaphoreType.DMA
    return pl.pallas_call(
        layer_kernel,
        out_shape=jax.ShapeDtypeStruct((ROWS, HALF), BF16),
        in_specs=[any_spec] * 11 + [vmem_spec] * 6,
        out_specs=any_spec,
        scratch_shapes=[
            pltpu.VMEM((2, 4, 4, 64, COLS), BF16),
            pltpu.VMEM((2, ROWS, HALF), BF16),
            pltpu.VMEM((ROWS, 2048), BF16),
            pltpu.VMEM((ROWS, 1536), BF16),
            pltpu.VMEM((ROWS, 256), F32),
            pltpu.VMEM((ROWS, 256), F32),
            pltpu.VMEM((ROWS, 512), BF16),
            pltpu.VMEM((8, ROWS, 256), BF16),
            pltpu.VMEM((8, ROWS, 256), BF16),
            pltpu.VMEM((ROWS, FF), BF16),
            pltpu.VMEM((4, ROWS, 256), BF16),
            pltpu.VMEM((4, ROWS, 256), BF16),
            pltpu.VMEM((4, ROWS, 256), BF16),
            dma((NSEM,)),
            dma((NSEM,)),
            dma((11,)),
            dma((13,)),
            dma((13,)),
            dma((4,)),
        ],
        compiler_params=pltpu.CompilerParams(
            collective_id=0, has_side_effects=True, vmem_limit_bytes=67043328
        ),
        name="layer",
    )(
        tokens,
        query_projection_weight,
        key_projection_weight,
        value_projection_weight,
        output_gate_weight,
        decay_projection_weight,
        mixer_result_matrix.T,
        up_linear_weight,
        up_gating_weight,
        down_projection_weight.T,
        added_fading_exponent,
        first_norm_gain[None],
        fading_shift_vector[None],
        per_head_gain[None],
        second_norm_gain[None],
        depthwise_taps,
        depthwise_bias,
    )


def solution(mesh):
    return jax.shard_map(
        local,
        mesh=mesh,
        in_specs=(
            P(("rep", "fs"), "tp"),
            P(),
            P("fs", "tp"),
            P("fs", "tp"),
            P("fs", "tp"),
            P("fs", "tp"),
            P("fs", "tp"),
            P("tp"),
            P(("rep", "fs"), "tp"),
            P(),
            P("tp", "fs"),
            P(),
            P("fs", "tp"),
            P("fs", "tp"),
            P(None, None, "tp"),
            P(None, "tp"),
            P("tp", "fs"),
        ),
        out_specs=P(("rep", "fs"), "tp"),
        check_vma=False,
    )
```

profile of v0, /device:TPU:1, one launch (start us, length us, event | category | flops | bytes accessed | tf_op | source)
XLA Modules:
  0.0 147.1 jit_solution(11285570649032181994)
XLA Ops:
  0.0 1.3 broadcast_in_dim.12.gain_one
  1.3 1.3 broadcast_in_dim.15.gain_two
  2.6 1.3 copy.18.taps
  3.9 140.5 %layer.1 = bf16[768,1024]{1,0:T(8,128)(2,1)} custom-call(bf16[768,1024]{1,0:T(8,128)(2,1)} %tokens.1, bf16[64,256]{1,0:T(8,128)(2,1)} %wq.1, bf16[64,256]{1,0:T(8,128)(2,1)} %wk.1, bf16[64,512]{1,0:T(8,128)(2,1)} %wv.1, bf16[64,512]{1,0:T(8,128)(2,1)} %wg.1, bf16[64,256]{1,0:T(8,128)(2,1)} %wd.1, bf16[64,512]{1,0:T(8,128)(2,1)} %bitcast.5, ...), custom_call_target="tpu_custom_call" | custom-call | tf_op jit(solution)/shard_map/layer/pallas_call | solution.py:523
  144.4 2.7 %copy.20 = bf16[768,1024]{1,0:T(8,128)(2,1)} copy(bf16[768,1024]{1,0:T(8,128)(2,1)} %layer.1) | data formatting | bytes 3145728
where the time goes:
time: 147 us
  Pallas kernels  141 us (96%)
  local copies, waits for them, and re-layouts  6.58 us (4%)
    pallas_call x1, Pallas kernels, local(): pl.pallas_call(layer_kernel, out_shape=jax.ShapeDtypeStruct((ROWS, HALF),...  141 us
    unnamed x2, local copies, waits for them, and re-layouts  4.01 us

commit v1 on v0

--- a/solution.py
+++ b/solution.py
@@ -7,7 +7,7 @@
 
 LANE = 128
 MESH = pl.DeviceIdType.MESH
-GROUPS = ((0, (6, 5, 3, 4)), (18, (7, 8, 5, 4)), (42, (4, 4, 2, 2)))
+GROUPS = ((0, (5, 6, 4, 3)), (18, (8, 7, 4, 5)), (42, (3, 3, 3, 3)))
 COLS = 54 * LANE
 CLASSES = (("x", 1, True), ("y", -1, True), ("x", 1, False), ("y", -1, False))
 NSEM = 144
@@ -112,42 +112,38 @@
             self.zkey(g, c, stage, off), self.piece(g, c, stage, off, z=1 - self.l)
         )
 
-    def step(self, g, s):
-        if s == 0:
-            for c in (0, 1):
+    def unit(self, g, c, k):
+        last = CLASSES[c][2]
+        if k == 0:
+            if last:
                 self.hop_one(g, c, 1)
-            for c in (2, 3, 0, 1):
-                self.zsend(g, c, 1, 0)
-        elif s == 1:
-            for c in (2, 3):
-                self.zrecv(g, c, 1, 0)
-                self.hop_one(g, c, 1)
-        elif s in (2, 6):
-            stage = 1 if s == 2 else 2
-            for c in (0, 1):
-                self.hop_two(g, c, stage)
+            self.zsend(g, c, 1, 0)
+        elif k == 1:
+            self.zrecv(g, c, 1, 0)
+            self.hop_one(g, c, 1)
+        elif k in (2, 3, 6, 7):
+            stage = 1 if k < 4 else 2
+            self.hop_two(g, c, stage)
+            if last:
                 self.zsend(g, c, stage, -1)
                 self.zsend(g, c, stage, 1)
-        elif s in (3, 7):
-            for c in (2, 3):
-                self.hop_two(g, c, 1 if s == 3 else 2)
-        elif s in (4, 8):
-            stage = 1 if s == 4 else 2
-            for c in (0, 1):
-                self.hop_end(g, c, stage)
-                if stage == 1:
-                    self.hop_one(g, c, 2)
-                self.zsend(g, c, stage, 2)
-        elif s == 5:
-            for c in (2, 3):
-                self.hop_end(g, c, 1)
-                self.hop_one(g, c, 2)
-        elif s == 9:
-            for c in (2, 3):
-                self.hop_end(g, c, 2)
-            for c in (0, 1):
-                for stage, off in ((1, 0), (1, -1), (1, 1), (1, 2), (2, -1), (2, 1), (2, 2)):
-                    self.zrecv(g, c, stage, off)
+        elif k in (4, 5):
+            self.hop_end(g, c, 1)
+            self.hop_one(g, c, 2)
+            if last:
+                self.zsend(g, c, 1, 2)
+        elif k == 8:
+            self.hop_end(g, c, 2)
+            self.zsend(g, c, 2, 2)
+
+    def gathered(self, g):
+        for c in (2, 3):
+            self.hop_end(g, c, 2)
+        for c in (0, 1):
+            for off in (0, -1, 1, 2):
+                self.zrecv(g, c, 1, off)
+            for off in (-1, 1, 2):
+                self.zrecv(g, c, 2, off)
 
     def enter(self):
         barrier = pltpu.get_barrier_semaphore()
@@ -158,43 +154,66 @@
     def partner(self):
         return (self.z // 2, self.l * 16 + self.y * 4 + self.x, 1 - self.tp)
 
-    def steps(self, todo):
-        for g, s in todo:
-            self.step(g, s)
-
-    def steps_in(self, i, plan):
-        for at, todo in plan.items():
-
-            @pl.when(i == at)
+    def steps(self, phase, i=0):
+        for todo in PLAN.get(phase, {}).get(i, ()):
+            self.unit(*todo)
+
+    def steps_in(self, i, phase, every=1, start=0):
+        for at in sorted(set(PLAN.get(phase, {})) - set(range(start))):
+
+            @pl.when(i == at * every + every - 1)
             def _():
-                self.steps(todo)
+                self.steps(phase, at)
 
     def leave(self):
         for key, (ref_args, dim, step) in self.sent.items():
             self.copy(key, self.piece(*ref_args), dim, step).wait_send()
 
 
+LIMIT = 58720256
 ROWS = 768
 SEQ = 256
 HALF = 1024
 NORM_EPS = 1e-06
+VALUE_DIM = 128
 SHARPNESS = 16.0
 MIX_AT, UP_AT, DOWN_AT, FF = 1792, 2304, 5376, 1536
-ROW_STEP = 16
+ROW_STEP = 64
+PER_UNIT = ROWS // ROW_STEP // 6
 F32, BF16 = jnp.float32, jnp.bfloat16
 
 PLAN = {
-    "open": [(0, 0)],
-    "tokens": [(0, 1)],
-    "norm": {8: [(0, 2)], 16: [(0, 3)], 32: [(0, 4), (0, 5), (1, 0)]},
-    "first": [(0, 6), (1, 1), (0, 7), (0, 8), (1, 2), (1, 3), (1, 4), (1, 5), (0, 9), (2, 0)],
-    "project": {5: [(1, 6), (2, 1)]},
-    "heads": {1: [(1, 7)], 3: [(2, 2)]},
-    "mix": {1: [(1, 8), (2, 3)], 5: [(2, 4)]},
-    "second": {0: [(2, 5)]},
-    "up_first": [(1, 9)],
-    "up": {1: [(2, 6)], 3: [(2, 7)], 4: [(2, 8)]},
-    "last": [(2, 9)],
+    'open': {
+        0: [(2, 1, 0), (0, 3, 0), (0, 1, 0), (0, 2, 0), (0, 0, 0), (2, 3, 0)],
+    },
+    'norm': {
+        0: [(1, 1, 0), (1, 0, 0), (0, 0, 2), (1, 2, 0), (0, 1, 2), (0, 3, 1), (0, 2, 1), (1, 0, 2), (2, 0, 0), (1, 1, 2), (0, 0, 4), (2, 2, 0), (0, 1, 4), (1, 3, 0), (0, 2, 3)],
+        1: [(0, 3, 3), (2, 3, 1), (0, 0, 6), (1, 0, 4), (1, 1, 4), (0, 0, 8), (2, 0, 2), (0, 1, 6), (2, 2, 1), (1, 3, 1), (1, 2, 1), (0, 1, 8)],
+        2: [(0, 2, 5), (2, 2, 3)],
+        3: [(2, 3, 3), (0, 3, 5), (1, 1, 6)],
+        4: [(1, 3, 3), (0, 2, 7), (1, 0, 6), (0, 3, 7), (2, 1, 2), (1, 1, 8), (1, 2, 3), (1, 3, 5)],
+    },
+    'project': {
+        0: [(1, 2, 5)],
+        4: [(2, 1, 4), (1, 0, 8)],
+    },
+    'heads': {
+        4: [(2, 0, 4)],
+    },
+    'mix': {
+        2: [(1, 3, 7)],
+        6: [(1, 2, 7)],
+    },
+    'mixed': {
+        0: [(2, 1, 6), (2, 0, 6)],
+    },
+    'second': {
+        4: [(2, 2, 5), (2, 3, 5)],
+    },
+    'up': {
+        2: [(2, 1, 8)],
+        3: [(2, 2, 7), (2, 0, 8), (2, 3, 7)],
+    },
 }
 
 
@@ -211,7 +230,7 @@
     scale = lax.rsqrt(total * (1.0 / 2048) + NORM_EPS)
     width = 2048 // len(parts)
     return [
-        (p * scale * gain_ref[:, i * width : (i + 1) * width].astype(F32)).astype(BF16)
+        (p * scale * gain_ref[:, i * width : (i + 1) * width]).astype(BF16)
         for i, p in enumerate(parts)
     ]
 
@@ -290,7 +309,7 @@
         values = qkvg[rows, pl.ds(pl.multiple_of(place + 512, LANE), LANE)]
         out = dot(scores.astype(BF16), values)
         scale = lax.rsqrt(jnp.mean(out * out, axis=-1, keepdims=True) + NORM_EPS)
-        out = out * scale * head_gain[...].astype(F32)
+        out = out * scale * head_gain[...]
         gate = qkvg[rows, pl.ds(pl.multiple_of(place + 1024, LANE), LANE)].astype(F32)
         out = out * (gate * jax.nn.sigmoid(gate))
         mixed[rows, pl.ds(place, LANE)] = out.astype(BF16)
@@ -323,6 +342,7 @@
     bias,
     out,
     full,
+    gains,
     tok,
     normed,
     qkvg,
@@ -334,16 +354,19 @@
     hidden,
     down_out,
     down_in,
-    result,
     send_sem,
     recv_sem,
     load_sem,
     pair_send,
     pair_recv,
-    out_sem,
 ):
     g = Gather(full, send_sem, recv_sem)
     tp = g.tp
+    gains[0:1] = gain_one[...].astype(F32)[None]
+    gains[1:2] = gain_two[...].astype(F32)[None]
+    gains[2:3, :VALUE_DIM] = head_gain[...].astype(F32)[None]
+    gain_one, gain_two = gains.at[0:1], gains.at[1:2]
+    head_gain = gains.at[2:3, :VALUE_DIM]
     own = full.at[g.l, g.y, g.x]
     loads = [pltpu.make_async_copy(tokens, tok.at[tp], load_sem.at[0])]
     at = 0
@@ -369,16 +392,13 @@
             device_id_type=MESH,
         )
 
-    for load in loads[1:7]:
+    for load in loads[1:]:
         load.wait()
-    for load in loads[7:]:
-        load.wait()
-    g.steps(PLAN["open"])
+    g.steps("open")
     loads[0].wait()
     swap_tokens = to_partner(tok.at[tp], tok.at[tp], 0)
     swap_tokens.start()
     fading_load.wait()
-    g.steps(PLAN["tokens"])
     to_partner(tok.at[tp], tok.at[1 - tp], 0).wait_recv()
 
     def first_norm(i, _):
@@ -386,28 +406,31 @@
         parts = normalize([tok[h, rows, :].astype(F32) for h in range(2)], gain_one)
         for h in range(2):
             normed[rows, h * HALF : (h + 1) * HALF] = parts[h]
-        g.steps_in(i, PLAN["norm"])
+        g.steps_in(i, "norm", PER_UNIT)
         return 0
 
     lax.fori_loop(0, ROWS // ROW_STEP, first_norm, 0)
-    g.steps(PLAN["first"])
+    g.gathered(0)
+    g.steps("got0")
 
     score = dot(normed[...], full[:, :, :, :, 1536:1792].reshape(2048, 256)) + shift[...]
     faded = jnp.minimum(score, 0.0) - jnp.log1p(jnp.exp(-jnp.abs(score)))
     decay[...] = faded * (1.0 / SHARPNESS) + fading[...]
+
+    g.steps("project")
 
     def project(j, _):
         cols = pl.ds(pl.multiple_of(j * 256, 256), 256)
         weight = full[:, :, :, :, cols].reshape(2048, 256)
         qkvg[:, cols] = dot(normed[...], weight).astype(BF16)
-        g.steps_in(j, PLAN["project"])
+        g.steps_in(j + 1, "project", 1, 1)
         return 0
 
     lax.fori_loop(0, 6, project, 0)
 
     def heads(i, _):
         head_pair(i // 2, lax.rem(i, 2), qkvg, decay, mixed, head_gain)
-        g.steps_in(i, PLAN["heads"])
+        g.steps_in(i, "heads")
         return 0
 
     lax.fori_loop(0, 6, heads, 0)
@@ -416,12 +439,13 @@
         weight = full[j // 4, lax.rem(j, 4), :, :, MIX_AT:UP_AT].reshape(256, 512)
         mix_out[j] = dot_nt(mixed[...], weight).astype(BF16)
         to_partner(mix_out.at[j], mix_in.at[j], 1 + j).start()
-        g.steps_in(j, PLAN["mix"])
+        g.steps_in(j, "mix")
         return 0
 
     lax.fori_loop(0, 8, mix, 0)
     for j in range(8):
         to_partner(mix_out.at[j], mix_in.at[j], 1 + j).wait_recv()
+    g.steps("mixed")
 
     def second_norm(i, _):
         rows = pl.ds(pl.multiple_of(i * ROW_STEP, ROW_STEP), ROW_STEP)
@@ -434,12 +458,13 @@
             parts.append(kept.astype(F32))
         for j, part in enumerate(normalize(parts, gain_two)):
             normed[rows, j * 256 : (j + 1) * 256] = part
-        g.steps_in(i, PLAN["second"])
+        g.steps_in(i, "second", PER_UNIT)
         return 0
 
     swap_tokens.wait_send()
     lax.fori_loop(0, ROWS // ROW_STEP, second_norm, 0)
-    g.steps(PLAN["up_first"])
+    g.gathered(1)
+    g.steps("got1")
 
     def up(j, _):
         cols = pl.ds(pl.multiple_of(j * 256, 256), 256)
@@ -448,7 +473,7 @@
             at = pl.multiple_of(UP_AT + half * FF + j * 256, 256)
             weight = full[:, :, :, :, pl.ds(at, 256)].reshape(2048, 256)
             parts.append(dot(normed[...], weight).astype(BF16))
-        tap = [taps[half, :, cols].astype(F32) for half in range(2)]
+        tap = [taps[:, half, cols].astype(F32) for half in range(2)]
         base = bias[:, cols].astype(F32)
         for s in range(ROWS // SEQ):
             rows = slice(s * SEQ, (s + 1) * SEQ)
@@ -456,11 +481,11 @@
                 smooth(parts[h][rows].astype(F32), tap[h], base[h : h + 1]) for h in range(2)
             )
             hidden[rows, cols] = (lin * (gate * jax.nn.sigmoid(gate))).astype(BF16)
-        g.steps_in(j, PLAN["up"])
+        g.steps_in(j, "up")
         return 0
 
     lax.fori_loop(0, FF // 256, up, 0)
-    g.steps(PLAN["last"])
+    g.gathered(2)
 
     def down_part(half, j):
         weight = full[half, j, :, :, DOWN_AT:COLS].reshape(256, FF)
@@ -472,21 +497,13 @@
         return 0
 
     lax.fori_loop(0, 4, down_theirs, 0)
-
-    def stored(j):
-        return pltpu.make_async_copy(
-            result.at[j],
-            out.at[:, pl.ds(pl.multiple_of(j * 256, 256), 256)],
-            out_sem.at[j],
-        )
 
     def down_mine(j, _):
         mine = down_part(tp, j).astype(F32)
         to_partner(down_out.at[j], down_in.at[j], 9 + j).wait_recv()
         cols = pl.ds(pl.multiple_of(j * 256, 256), 256)
         summed = mine + down_in[j].astype(F32)
-        result[j] = (tok[tp, :, cols].astype(F32) + summed).astype(BF16)
-        stored(j).start()
+        out[:, cols] = (tok[tp, :, cols].astype(F32) + summed).astype(BF16)
         return 0
 
     lax.fori_loop(0, 4, down_mine, 0)
@@ -494,7 +511,6 @@
         to_partner(mix_out.at[j], mix_in.at[j], 1 + j).wait_send()
     for j in range(4):
         to_partner(down_out.at[j], down_in.at[j], 9 + j).wait_send()
-        stored(j).wait()
     g.leave()
 
 
@@ -522,11 +538,12 @@
     dma = pltpu.SemaphoreType.DMA
     return pl.pallas_call(
         layer_kernel,
-        out_shape=jax.ShapeDtypeStruct((ROWS, HALF), BF16),
+        out_shape=pltpu.VMEM((ROWS, HALF), BF16),
         in_specs=[any_spec] * 11 + [vmem_spec] * 6,
-        out_specs=any_spec,
+        out_specs=vmem_spec,
         scratch_shapes=[
             pltpu.VMEM((2, 4, 4, 64, COLS), BF16),
+            pltpu.VMEM((8, 2048), F32),
             pltpu.VMEM((2, ROWS, HALF), BF16),
             pltpu.VMEM((ROWS, 2048), BF16),
             pltpu.VMEM((ROWS, 1536), BF16),
@@ -538,16 +555,14 @@
             pltpu.VMEM((ROWS, FF), BF16),
             pltpu.VMEM((4, ROWS, 256), BF16),
             pltpu.VMEM((4, ROWS, 256), BF16),
-            pltpu.VMEM((4, ROWS, 256), BF16),
             dma((NSEM,)),
             dma((NSEM,)),
             dma((11,)),
             dma((13,)),
             dma((13,)),
-            dma((4,)),
         ],
         compiler_params=pltpu.CompilerParams(
-            collective_id=0, has_side_effects=True, vmem_limit_bytes=67043328
+            collective_id=0, has_side_effects=True, vmem_limit_bytes=LIMIT
         ),
         name="layer",
     )(
@@ -562,11 +577,11 @@
         up_gating_weight,
         down_projection_weight.T,
         added_fading_exponent,
-        first_norm_gain[None],
+        first_norm_gain,
         fading_shift_vector[None],
-        per_head_gain[None],
-        second_norm_gain[None],
-        depthwise_taps,
+        per_head_gain,
+        second_norm_gain,
+        depthwise_taps.transpose(1, 0, 2),
         depthwise_bias,
     )
 

time: 147 us -> 126 us (0.86)
  Pallas kernels: 141 us -> 124 us
  local copies, waits for them, and re-layouts: 6.58 us -> 1.15 us
    pallas_call x1, Pallas kernels: 141 us -> 124 us  [local(): pl.pallas_call(layer_kernel, out_shape=pltpu.VMEM((ROWS, HALF), BF16), in...]
    unnamed x2 -> x1, local copies, waits for them, and re-layouts: 4.01 us -> 1.15 us
    broadcast_in_dim x2 -> x0, local copies, waits for them, and re-layouts: 2.57 us -> none  [the longest x1 1.29 us: local(): second_norm_gain[None]]
where the time goes in v1:
time: 126 us; the launch traced here: 125 us
  Pallas kernels  124 us (98%)
    pallas_call x1, Pallas kernels, local(): pl.pallas_call(layer_kernel, out_shape=pltpu.VMEM((ROWS, HALF), BF16), in...  124 us

profile of v1, /device:TPU:1, one launch (start us, length us, event | category | flops | bytes accessed | tf_op | source)
XLA Modules:
  0.0 125.3 jit_solution(15614441675904934649)
XLA Ops:
  0.0 124.2 %layer.1 = bf16[768,1024]{1,0:T(8,128)(2,1)S(1)} custom-call(bf16[768,1024]{1,0:T(8,128)(2,1)} %tokens.1, bf16[64,256]{1,0:T(8,128)(2,1)} %wq.1, bf16[64,256]{1,0:T(8,128)(2,1)} %wk.1, bf16[64,512]{1,0:T(8,128)(2,1)} %wv.1, bf16[64,512]{1,0:T(8,128)(2,1)} %wg.1, bf16[64,256]{1,0:T(8,128)(2,1)} %wd.1, bf16[64,512]{1,0:T(8,128)(2,1)} %bitcast.5, ...), custom_call_target="tpu_custom_call" | custom-call | tf_op jit(solution)/shard_map/layer/pallas_call | solution.py:539
  124.2 1.1 copy.19

commit v2 on v1

--- a/solution.py
+++ b/solution.py
@@ -7,7 +7,7 @@
 
 LANE = 128
 MESH = pl.DeviceIdType.MESH
-GROUPS = ((0, (5, 6, 4, 3)), (18, (8, 7, 4, 5)), (42, (3, 3, 3, 3)))
+GROUPS = ((0, (6, 7, 3, 2)), (18, (8, 7, 4, 5)), (42, (3, 3, 3, 3)))
 COLS = 54 * LANE
 CLASSES = (("x", 1, True), ("y", -1, True), ("x", 1, False), ("y", -1, False))
 NSEM = 144
@@ -136,10 +136,11 @@
             self.hop_end(g, c, 2)
             self.zsend(g, c, 2, 2)
 
-    def gathered(self, g):
-        for c in (2, 3):
-            self.hop_end(g, c, 2)
-        for c in (0, 1):
+    def gathered(self, g, classes=(2, 3, 0, 1)):
+        for c in classes:
+            if not CLASSES[c][2]:
+                self.hop_end(g, c, 2)
+                continue
             for off in (0, -1, 1, 2):
                 self.zrecv(g, c, 1, off)
             for off in (-1, 1, 2):
@@ -170,7 +171,7 @@
             self.copy(key, self.piece(*ref_args), dim, step).wait_send()
 
 
-LIMIT = 58720256
+LIMIT = 65011712
 ROWS = 768
 SEQ = 256
 HALF = 1024
@@ -178,41 +179,44 @@
 VALUE_DIM = 128
 SHARPNESS = 16.0
 MIX_AT, UP_AT, DOWN_AT, FF = 1792, 2304, 5376, 1536
-ROW_STEP = 64
+ROW_STEP = 128
 PER_UNIT = ROWS // ROW_STEP // 6
 F32, BF16 = jnp.float32, jnp.bfloat16
 
 PLAN = {
     'open': {
-        0: [(2, 1, 0), (0, 3, 0), (0, 1, 0), (0, 2, 0), (0, 0, 0), (2, 3, 0)],
+        0: [(0, 3, 0), (0, 0, 0), (0, 1, 0), (0, 2, 0)],
     },
     'norm': {
-        0: [(1, 1, 0), (1, 0, 0), (0, 0, 2), (1, 2, 0), (0, 1, 2), (0, 3, 1), (0, 2, 1), (1, 0, 2), (2, 0, 0), (1, 1, 2), (0, 0, 4), (2, 2, 0), (0, 1, 4), (1, 3, 0), (0, 2, 3)],
-        1: [(0, 3, 3), (2, 3, 1), (0, 0, 6), (1, 0, 4), (1, 1, 4), (0, 0, 8), (2, 0, 2), (0, 1, 6), (2, 2, 1), (1, 3, 1), (1, 2, 1), (0, 1, 8)],
-        2: [(0, 2, 5), (2, 2, 3)],
-        3: [(2, 3, 3), (0, 3, 5), (1, 1, 6)],
-        4: [(1, 3, 3), (0, 2, 7), (1, 0, 6), (0, 3, 7), (2, 1, 2), (1, 1, 8), (1, 2, 3), (1, 3, 5)],
+        0: [(1, 0, 0), (1, 3, 0), (1, 1, 0), (0, 0, 2), (0, 1, 2), (0, 2, 1)],
+        2: [(1, 2, 0), (0, 3, 1), (1, 0, 2), (2, 3, 0), (2, 2, 0), (1, 1, 2), (0, 0, 4), (0, 1, 4), (0, 3, 3)],
+        3: [(1, 3, 1), (0, 2, 3)],
+        4: [(0, 0, 6), (1, 1, 4), (0, 3, 5), (0, 2, 5), (0, 1, 6), (2, 1, 0), (2, 2, 1), (2, 0, 0), (1, 2, 1), (0, 0, 8), (1, 0, 4), (0, 3, 7), (1, 3, 3)],
+        5: [(0, 1, 8), (0, 2, 7), (1, 1, 6), (1, 0, 6), (1, 2, 3), (1, 3, 5), (2, 3, 1), (1, 1, 8)],
     },
     'project': {
-        0: [(1, 2, 5)],
-        4: [(2, 1, 4), (1, 0, 8)],
+        0: [(2, 1, 2), (1, 2, 5), (1, 0, 8)],
+        2: [(2, 0, 2), (2, 2, 3)],
+        3: [(2, 3, 3)],
     },
     'heads': {
+        0: [(2, 1, 4)],
         4: [(2, 0, 4)],
     },
     'mix': {
-        2: [(1, 3, 7)],
-        6: [(1, 2, 7)],
+        0: [(1, 3, 7)],
+        4: [(2, 3, 5)],
+        6: [(1, 2, 7), (2, 2, 5)],
     },
     'mixed': {
-        0: [(2, 1, 6), (2, 0, 6)],
-    },
-    'second': {
-        4: [(2, 2, 5), (2, 3, 5)],
+        0: [(2, 1, 6)],
+    },
+    'got1': {
+        0: [(2, 0, 6)],
     },
     'up': {
-        2: [(2, 1, 8)],
-        3: [(2, 2, 7), (2, 0, 8), (2, 3, 7)],
+        2: [(2, 3, 7), (2, 2, 7)],
+        3: [(2, 1, 8), (2, 0, 8)],
     },
 }
 
@@ -354,6 +358,7 @@
     hidden,
     down_out,
     down_in,
+    partial,
     send_sem,
     recv_sem,
     load_sem,
@@ -362,11 +367,6 @@
 ):
     g = Gather(full, send_sem, recv_sem)
     tp = g.tp
-    gains[0:1] = gain_one[...].astype(F32)[None]
-    gains[1:2] = gain_two[...].astype(F32)[None]
-    gains[2:3, :VALUE_DIM] = head_gain[...].astype(F32)[None]
-    gain_one, gain_two = gains.at[0:1], gains.at[1:2]
-    head_gain = gains.at[2:3, :VALUE_DIM]
     own = full.at[g.l, g.y, g.x]
     loads = [pltpu.make_async_copy(tokens, tok.at[tp], load_sem.at[0])]
     at = 0
@@ -380,6 +380,11 @@
     for load in loads:
         load.start()
     fading_load.start()
+    gains[0:1] = gain_one[...].astype(F32)[None]
+    gains[1:2] = gain_two[...].astype(F32)[None]
+    gains[2:3, :VALUE_DIM] = head_gain[...].astype(F32)[None]
+    gain_one, gain_two = gains.at[0:1], gains.at[1:2]
+    head_gain = gains.at[2:3, :VALUE_DIM]
     g.enter()
 
     def to_partner(src, dst, n):
@@ -485,31 +490,43 @@
         return 0
 
     lax.fori_loop(0, FF // 256, up, 0)
-    g.gathered(2)
-
-    def down_part(half, j):
-        weight = full[half, j, :, :, DOWN_AT:COLS].reshape(256, FF)
-        return dot_nt(hidden[...], weight).astype(BF16)
+    late = sum(GROUPS[2][1][:2]) * LANE
+
+    def down_part(half, j, low, high):
+        pair = pl.ds(pl.multiple_of(2 * j, 2), 2)
+        weight = full[half, pair, :, :, DOWN_AT + low : DOWN_AT + high]
+        return dot_nt(hidden[:, low:high], weight.reshape(512, high - low))
+
+    def down_early(i, _):
+        half = lax.rem(1 - tp + i // 2, 2)
+        partial[i] = down_part(half, lax.rem(i, 2), late, FF)
+        g.steps_in(i, "downa")
+        return 0
+
+    g.gathered(2, (2, 3))
+    g.steps("got2a")
+    lax.fori_loop(0, 4, down_early, 0)
+    g.gathered(2, (0, 1))
 
     def down_theirs(j, _):
-        down_out[j] = down_part(1 - tp, j)
+        down_out[j] = (partial[j] + down_part(1 - tp, j, 0, late)).astype(BF16)
         to_partner(down_out.at[j], down_in.at[j], 9 + j).start()
         return 0
 
-    lax.fori_loop(0, 4, down_theirs, 0)
+    lax.fori_loop(0, 2, down_theirs, 0)
 
     def down_mine(j, _):
-        mine = down_part(tp, j).astype(F32)
+        mine = (partial[j + 2] + down_part(tp, j, 0, late)).astype(BF16).astype(F32)
         to_partner(down_out.at[j], down_in.at[j], 9 + j).wait_recv()
-        cols = pl.ds(pl.multiple_of(j * 256, 256), 256)
+        cols = pl.ds(pl.multiple_of(j * 512, 512), 512)
         summed = mine + down_in[j].astype(F32)
         out[:, cols] = (tok[tp, :, cols].astype(F32) + summed).astype(BF16)
         return 0
 
-    lax.fori_loop(0, 4, down_mine, 0)
+    lax.fori_loop(0, 2, down_mine, 0)
     for j in range(8):
         to_partner(mix_out.at[j], mix_in.at[j], 1 + j).wait_send()
-    for j in range(4):
+    for j in range(2):
         to_partner(down_out.at[j], down_in.at[j], 9 + j).wait_send()
     g.leave()
 
@@ -553,13 +570,14 @@
             pltpu.VMEM((8, ROWS, 256), BF16),
             pltpu.VMEM((8, ROWS, 256), BF16),
             pltpu.VMEM((ROWS, FF), BF16),
-            pltpu.VMEM((4, ROWS, 256), BF16),
-            pltpu.VMEM((4, ROWS, 256), BF16),
+            pltpu.VMEM((2, ROWS, 512), BF16),
+            pltpu.VMEM((2, ROWS, 512), BF16),
+            pltpu.VMEM((4, ROWS, 512), F32),
             dma((NSEM,)),
             dma((NSEM,)),
             dma((11,)),
-            dma((13,)),
-            dma((13,)),
+            dma((11,)),
+            dma((11,)),
         ],
         compiler_params=pltpu.CompilerParams(
             collective_id=0, has_side_effects=True, vmem_limit_bytes=LIMIT

time: 126 us -> 123 us (0.976)
  Pallas kernels: 124 us -> 122 us
    pallas_call x1, Pallas kernels: 124 us -> 122 us  [local(): pl.pallas_call(layer_kernel, out_shape=pltpu.VMEM((ROWS, HALF), BF16), in...]
where the time goes in v2:
time: 123 us
  Pallas kernels  122 us (99%)
    pallas_call x1, Pallas kernels, local(): pl.pallas_call(layer_kernel, out_shape=pltpu.VMEM((ROWS, HALF), BF16), in...  122 us

profile of v2, /device:TPU:1, one launch (start us, length us, event | category | flops | bytes accessed | tf_op | source)
XLA Modules:
  0.0 123.3 jit_solution(2156341103469799413)
XLA Ops:
  0.0 122.1 %layer.1 = bf16[768,1024]{1,0:T(8,128)(2,1)S(1)} custom-call(bf16[768,1024]{1,0:T(8,128)(2,1)} %tokens.1, bf16[64,256]{1,0:T(8,128)(2,1)} %wq.1, bf16[64,256]{1,0:T(8,128)(2,1)} %wk.1, bf16[64,512]{1,0:T(8,128)(2,1)} %wv.1, bf16[64,512]{1,0:T(8,128)(2,1)} %wg.1, bf16[64,256]{1,0:T(8,128)(2,1)} %wd.1, bf16[64,512]{1,0:T(8,128)(2,1)} %bitcast.5, ...), custom_call_target="tpu_custom_call" | custom-call | tf_op jit(solution)/shard_map/layer/pallas_call | solution.py:556
  122.1 1.1 copy.19

commit v3 on v2

--- a/solution.py
+++ b/solution.py
@@ -7,7 +7,7 @@
 
 LANE = 128
 MESH = pl.DeviceIdType.MESH
-GROUPS = ((0, (6, 7, 3, 2)), (18, (8, 7, 4, 5)), (42, (3, 3, 3, 3)))
+GROUPS = ((0, (6, 6, 3, 3)), (18, (8, 8, 4, 4)), (42, (3, 3, 3, 3)))
 COLS = 54 * LANE
 CLASSES = (("x", 1, True), ("y", -1, True), ("x", 1, False), ("y", -1, False))
 NSEM = 144
@@ -159,8 +159,8 @@
         for todo in PLAN.get(phase, {}).get(i, ()):
             self.unit(*todo)
 
-    def steps_in(self, i, phase, every=1, start=0):
-        for at in sorted(set(PLAN.get(phase, {})) - set(range(start))):
+    def steps_in(self, i, phase, every=1, start=0, stop=99):
+        for at in sorted(set(PLAN.get(phase, {})) & set(range(start, stop))):
 
             @pl.when(i == at * every + every - 1)
             def _():
@@ -185,38 +185,40 @@
 
 PLAN = {
     'open': {
-        0: [(0, 3, 0), (0, 0, 0), (0, 1, 0), (0, 2, 0)],
+        0: [(2, 3, 0), (0, 2, 0), (0, 0, 0), (0, 3, 0), (0, 1, 0), (1, 2, 0), (2, 1, 0), (1, 0, 0), (1, 1, 0), (0, 0, 2), (0, 2, 1), (1, 3, 0), (0, 1, 2)],
     },
     'norm': {
-        0: [(1, 0, 0), (1, 3, 0), (1, 1, 0), (0, 0, 2), (0, 1, 2), (0, 2, 1)],
-        2: [(1, 2, 0), (0, 3, 1), (1, 0, 2), (2, 3, 0), (2, 2, 0), (1, 1, 2), (0, 0, 4), (0, 1, 4), (0, 3, 3)],
-        3: [(1, 3, 1), (0, 2, 3)],
-        4: [(0, 0, 6), (1, 1, 4), (0, 3, 5), (0, 2, 5), (0, 1, 6), (2, 1, 0), (2, 2, 1), (2, 0, 0), (1, 2, 1), (0, 0, 8), (1, 0, 4), (0, 3, 7), (1, 3, 3)],
-        5: [(0, 1, 8), (0, 2, 7), (1, 1, 6), (1, 0, 6), (1, 2, 3), (1, 3, 5), (2, 3, 1), (1, 1, 8)],
+        0: [(0, 3, 1), (2, 2, 0), (2, 0, 0)],
+        1: [(2, 1, 2), (1, 2, 1), (0, 0, 4), (1, 1, 2), (0, 2, 3), (0, 3, 3)],
+        2: [(0, 1, 4), (0, 2, 5), (1, 0, 2)],
+        3: [(1, 3, 1), (2, 0, 2), (0, 3, 5), (0, 1, 6), (0, 0, 6), (1, 0, 4)],
+        4: [(1, 1, 4)],
+        5: [(0, 0, 8), (1, 3, 3), (1, 2, 3), (0, 1, 8), (0, 3, 7), (2, 2, 1), (0, 2, 7), (1, 3, 5), (1, 1, 6), (1, 2, 5), (1, 0, 6)],
     },
     'project': {
-        0: [(2, 1, 2), (1, 2, 5), (1, 0, 8)],
-        2: [(2, 0, 2), (2, 2, 3)],
-        3: [(2, 3, 3)],
+        6: [(2, 3, 1)],
     },
     'heads': {
-        0: [(2, 1, 4)],
-        4: [(2, 0, 4)],
+        1: [(1, 2, 7), (2, 2, 3)],
+        4: [(1, 3, 7)],
     },
     'mix': {
-        0: [(1, 3, 7)],
-        4: [(2, 3, 5)],
-        6: [(1, 2, 7), (2, 2, 5)],
-    },
-    'mixed': {
+        2: [(2, 1, 4), (1, 0, 8)],
+        4: [(2, 3, 3), (1, 1, 8), (2, 0, 4)],
+    },
+    'second': {
+        0: [(2, 2, 5)],
+        1: [(2, 3, 5)],
+    },
+    'up': {
+        0: [(2, 0, 6)],
+        4: [(2, 1, 8), (2, 0, 8)],
+    },
+    'got1b': {
         0: [(2, 1, 6)],
     },
-    'got1': {
-        0: [(2, 0, 6)],
-    },
-    'up': {
-        2: [(2, 3, 7), (2, 2, 7)],
-        3: [(2, 1, 8), (2, 0, 8)],
+    'got1c': {
+        0: [(2, 3, 7), (2, 2, 7)],
     },
 }
 
@@ -369,14 +371,18 @@
     tp = g.tp
     own = full.at[g.l, g.y, g.x]
     loads = [pltpu.make_async_copy(tokens, tok.at[tp], load_sem.at[0])]
+    parts = [(w, 0, w.shape[1]) for w in (wq, wk, wv, wg, wd, mix_t)]
+    parts += [(w, at, 256) for at in range(0, FF, 256) for w in (up_lin, up_gate)]
+    parts += [(down_t, 0, FF)]
     at = 0
-    for n, w in enumerate((wq, wk, wv, wg, wd, mix_t, up_lin, up_gate, down_t)):
-        width = w.shape[1]
+    for n, (w, first, width) in enumerate(parts):
         loads.append(
-            pltpu.make_async_copy(w, own.at[:, pl.ds(at, width)], load_sem.at[n + 1])
+            pltpu.make_async_copy(
+                w.at[:, pl.ds(first, width)], own.at[:, pl.ds(at, width)], load_sem.at[n + 1]
+            )
         )
         at += width
-    fading_load = pltpu.make_async_copy(added, fading, load_sem.at[10])
+    fading_load = pltpu.make_async_copy(added, fading, load_sem.at[20])
     for load in loads:
         load.start()
     fading_load.start()
@@ -399,10 +405,15 @@
 
     for load in loads[1:]:
         load.wait()
-    g.steps("open")
+    opening = PLAN["open"][0]
+    sends = next((n for n, todo in enumerate(opening) if todo[2]), len(opening))
+    for todo in opening[:sends]:
+        g.unit(*todo)
     loads[0].wait()
     swap_tokens = to_partner(tok.at[tp], tok.at[tp], 0)
     swap_tokens.start()
+    for todo in opening[sends:]:
+        g.unit(*todo)
     fading_load.wait()
     to_partner(tok.at[tp], tok.at[1 - tp], 0).wait_recv()
 
@@ -468,16 +479,12 @@
 
     swap_tokens.wait_send()
     lax.fori_loop(0, ROWS // ROW_STEP, second_norm, 0)
-    g.gathered(1)
-    g.steps("got1")
-
     def up(j, _):
         cols = pl.ds(pl.multiple_of(j * 256, 256), 256)
-        parts = []
-        for half in range(2):
-            at = pl.multiple_of(UP_AT + half * FF + j * 256, 256)
-            weight = full[:, :, :, :, pl.ds(at, 256)].reshape(2048, 256)
-            parts.append(dot(normed[...], weight).astype(BF16))
+        at = pl.multiple_of(UP_AT + j * 512, 256)
+        weight = full[:, :, :, :, pl.ds(at, 512)].reshape(2048, 512)
+        both = dot(normed[...], weight).astype(BF16)
+        parts = [both[:, :256], both[:, 256:]]
         tap = [taps[:, half, cols].astype(F32) for half in range(2)]
         base = bias[:, cols].astype(F32)
         for s in range(ROWS // SEQ):
@@ -486,10 +493,25 @@
                 smooth(parts[h][rows].astype(F32), tap[h], base[h : h + 1]) for h in range(2)
             )
             hidden[rows, cols] = (lin * (gate * jax.nn.sigmoid(gate))).astype(BF16)
-        g.steps_in(j, "up")
-        return 0
-
-    lax.fori_loop(0, FF // 256, up, 0)
+        return 0
+
+    done = 0
+    for phase, classes, chunks in (
+        ("got1a", (2, 3), (4, 6)),
+        ("got1b", (0,), (0, 2)),
+        ("got1c", (1,), (2, 4)),
+    ):
+        g.gathered(1, classes)
+        g.steps(phase)
+
+        def piece(j, _, shift=done - chunks[0], at=done):
+            up(j, 0)
+            g.steps_in(j + shift, "up", 1, at, at + 2)
+            return 0
+
+        lax.fori_loop(*chunks, piece, 0)
+        done += 2
+
     late = sum(GROUPS[2][1][:2]) * LANE
 
     def down_part(half, j, low, high):
@@ -575,7 +597,7 @@
             pltpu.VMEM((4, ROWS, 512), F32),
             dma((NSEM,)),
             dma((NSEM,)),
-            dma((11,)),
+            dma((21,)),
             dma((11,)),
             dma((11,)),
         ],

time: 123 us -> 120 us (0.976)
  Pallas kernels: 122 us -> 119 us
    pallas_call x1, Pallas kernels: 122 us -> 119 us  [local(): pl.pallas_call(layer_kernel, out_shape=pltpu.VMEM((ROWS, HALF), BF16), in...]
where the time goes in v3:
time: 120 us
  Pallas kernels  119 us (99%)
    pallas_call x1, Pallas kernels, local(): pl.pallas_call(layer_kernel, out_shape=pltpu.VMEM((ROWS, HALF), BF16), in...  119 us

profile of v3, /device:TPU:1, one launch (start us, length us, event | category | flops | bytes accessed | tf_op | source)
XLA Modules:
  0.0 120.2 jit_solution(8435261864202592890)
XLA Ops:
  0.0 119.0 %layer.1 = bf16[768,1024]{1,0:T(8,128)(2,1)S(1)} custom-call(bf16[768,1024]{1,0:T(8,128)(2,1)} %tokens.1, bf16[64,256]{1,0:T(8,128)(2,1)} %wq.1, bf16[64,256]{1,0:T(8,128)(2,1)} %wk.1, bf16[64,512]{1,0:T(8,128)(2,1)} %wv.1, bf16[64,512]{1,0:T(8,128)(2,1)} %wg.1, bf16[64,256]{1,0:T(8,128)(2,1)} %wd.1, bf16[64,512]{1,0:T(8,128)(2,1)} %bitcast.5, ...), custom_call_target="tpu_custom_call" | custom-call | tf_op jit(solution)/shard_map/layer/pallas_call | solution.py:578
  119.0 1.1 copy.19

commit v4 on v3

--- a/solution.py
+++ b/solution.py
@@ -10,7 +10,7 @@
 GROUPS = ((0, (6, 6, 3, 3)), (18, (8, 8, 4, 4)), (42, (3, 3, 3, 3)))
 COLS = 54 * LANE
 CLASSES = (("x", 1, True), ("y", -1, True), ("x", 1, False), ("y", -1, False))
-NSEM = 144
+NSEM = 168
 
 
 class Gather:
@@ -81,18 +81,29 @@
         return first if stage == 1 else ("y" if first == "x" else "x")
 
     def hop_one(self, g, c, stage):
-        own = (g, c, stage, 0)
-        self.send((g, c, stage, "f1"), own, self.dim(c, stage), 1)
-        self.send((g, c, stage, "b1"), own, self.dim(c, stage), -1)
+        d = self.dim(c, stage)
+        for late in range(stage):
+            for name, first, to in (("f1", 0, 1), ("b1", 1, -1)):
+                half = None if stage == 1 else (first + late) % 2
+                self.send((g, c, stage, name, late), (g, c, stage, 0, half), d, to)
 
     def hop_two(self, g, c, stage):
         d = self.dim(c, stage)
-        self.recv((g, c, stage, "f1"), self.piece(g, c, stage, -1))
-        self.send((g, c, stage, "f2"), (g, c, stage, -1, 0), d, 1)
-        self.recv((g, c, stage, "b1"), self.piece(g, c, stage, 1))
-        self.send((g, c, stage, "b2"), (g, c, stage, 1, 1), d, -1)
+        for name, onward, half, off in (("f1", "f2", 0, -1), ("b1", "b2", 1, 1)):
+            whole = None if stage == 1 else half
+            self.recv((g, c, stage, name, 0), self.piece(g, c, stage, off, whole))
+            self.send((g, c, stage, onward), (g, c, stage, off, half), d, -off)
+        if CLASSES[c][2]:
+            self.hop_rest(g, c, stage)
+
+    def hop_rest(self, g, c, stage):
+        if stage == 2:
+            self.recv((g, c, stage, "f1", 1), self.piece(g, c, stage, -1, 1))
+            self.recv((g, c, stage, "b1", 1), self.piece(g, c, stage, 1, 0))
 
     def hop_end(self, g, c, stage):
+        if not CLASSES[c][2]:
+            self.hop_rest(g, c, stage)
         self.recv((g, c, stage, "f2"), self.piece(g, c, stage, 2, 0))
         self.recv((g, c, stage, "b2"), self.piece(g, c, stage, 2, 1))
 
@@ -185,40 +196,39 @@
 
 PLAN = {
     'open': {
-        0: [(2, 3, 0), (0, 2, 0), (0, 0, 0), (0, 3, 0), (0, 1, 0), (1, 2, 0), (2, 1, 0), (1, 0, 0), (1, 1, 0), (0, 0, 2), (0, 2, 1), (1, 3, 0), (0, 1, 2)],
+        0: [(0, 2, 0), (0, 0, 0), (2, 2, 0), (0, 3, 0), (0, 1, 0)],
     },
     'norm': {
-        0: [(0, 3, 1), (2, 2, 0), (2, 0, 0)],
-        1: [(2, 1, 2), (1, 2, 1), (0, 0, 4), (1, 1, 2), (0, 2, 3), (0, 3, 3)],
-        2: [(0, 1, 4), (0, 2, 5), (1, 0, 2)],
-        3: [(1, 3, 1), (2, 0, 2), (0, 3, 5), (0, 1, 6), (0, 0, 6), (1, 0, 4)],
-        4: [(1, 1, 4)],
-        5: [(0, 0, 8), (1, 3, 3), (1, 2, 3), (0, 1, 8), (0, 3, 7), (2, 2, 1), (0, 2, 7), (1, 3, 5), (1, 1, 6), (1, 2, 5), (1, 0, 6)],
-    },
-    'project': {
-        6: [(2, 3, 1)],
+        0: [(1, 1, 0), (2, 3, 0), (1, 2, 0), (1, 3, 0), (2, 1, 0), (1, 0, 0), (2, 0, 0)],
+        1: [(0, 0, 2), (0, 3, 1)],
+        2: [(0, 1, 2), (0, 2, 1), (1, 2, 1), (1, 1, 2)],
+        3: [(0, 0, 4), (0, 1, 4), (1, 2, 3), (0, 2, 3), (1, 0, 2), (1, 3, 1), (0, 3, 3), (0, 0, 6), (0, 1, 6), (0, 3, 5), (0, 2, 5), (1, 3, 3), (1, 0, 4), (1, 1, 4), (0, 1, 8), (0, 2, 7), (0, 0, 8), (0, 3, 7), (2, 3, 1), (2, 2, 1), (2, 0, 2), (1, 0, 6)],
+        4: [(2, 1, 2), (1, 1, 6)],
+    },
+    'got0': {
+        0: [(1, 2, 5), (1, 3, 5)],
     },
     'heads': {
-        1: [(1, 2, 7), (2, 2, 3)],
-        4: [(1, 3, 7)],
+        1: [(2, 3, 3)],
+        2: [(1, 1, 8)],
+        3: [(1, 2, 7), (1, 3, 7), (2, 2, 3)],
+        5: [(1, 0, 8)],
     },
     'mix': {
-        2: [(2, 1, 4), (1, 0, 8)],
-        4: [(2, 3, 3), (1, 1, 8), (2, 0, 4)],
+        0: [(2, 1, 4)],
+        1: [(2, 0, 4)],
+        6: [(2, 3, 5)],
     },
     'second': {
-        0: [(2, 2, 5)],
-        1: [(2, 3, 5)],
+        4: [(2, 2, 5)],
     },
     'up': {
-        0: [(2, 0, 6)],
-        4: [(2, 1, 8), (2, 0, 8)],
+        1: [(2, 0, 6)],
+        2: [(2, 3, 7), (2, 2, 7)],
+        4: [(2, 0, 8), (2, 1, 8)],
     },
     'got1b': {
         0: [(2, 1, 6)],
-    },
-    'got1c': {
-        0: [(2, 3, 7), (2, 2, 7)],
     },
 }
 

time: 120 us -> 123 us (1.025)
  Pallas kernels: 119 us -> 121 us
    pallas_call x1, Pallas kernels: 119 us -> 121 us  [local(): pl.pallas_call(layer_kernel, out_shape=pltpu.VMEM((ROWS, HALF), BF16), in...]
where the time goes in v4:
time: 123 us; the launch traced here: 122 us
  Pallas kernels  121 us (98%)
    pallas_call x1, Pallas kernels, local(): pl.pallas_call(layer_kernel, out_shape=pltpu.VMEM((ROWS, HALF), BF16), in...  121 us

profile of v4, /device:TPU:1, one launch (start us, length us, event | category | flops | bytes accessed | tf_op | source)
XLA Modules:
  0.0 122.4 jit_solution(7427020079485333321)
XLA Ops:
  0.0 121.2 %layer.1 = bf16[768,1024]{1,0:T(8,128)(2,1)S(1)} custom-call(bf16[768,1024]{1,0:T(8,128)(2,1)} %tokens.1, bf16[64,256]{1,0:T(8,128)(2,1)} %wq.1, bf16[64,256]{1,0:T(8,128)(2,1)} %wk.1, bf16[64,512]{1,0:T(8,128)(2,1)} %wv.1, bf16[64,512]{1,0:T(8,128)(2,1)} %wg.1, bf16[64,256]{1,0:T(8,128)(2,1)} %wd.1, bf16[64,512]{1,0:T(8,128)(2,1)} %bitcast.5, ...), custom_call_target="tpu_custom_call" | custom-call | tf_op jit(solution)/shard_map/layer/pallas_call | solution.py:588
  121.2 1.1 copy.19
